TPU v7x, 32 devices: a whole 2x2x4 slice. The times are simulated.
32 devices in a mesh: sp: 16 (over z, y, x), tp: 2 (over core).
Axes of the slice: x: 2, y: 2, z: 4, core: 2. Of those that a mesh axis runs over, the one named last changes fastest.
Arguments:
- query_one: bfloat16 [2048, 1024], P('sp', 'tp'), may hold values from -6 to 6
- key_one: bfloat16 [2048, 1024], P('sp', 'tp'), may hold values from -6 to 6
- query_two: bfloat16 [2048, 512], P('sp', 'tp'), may hold values from -6 to 6
- key_two: bfloat16 [2048, 512], P('sp', 'tp'), may hold values from -6 to 6
- values: bfloat16 [2048, 2048], P('sp', 'tp'), may hold values from -6 to 6
- out_gate: bfloat16 [2048, 2048], P('sp', 'tp'), may hold values from -6 to 6
- in_gate: float32 [16, 2048], P('tp', 'sp'), may hold values from -3 to 150
- forget_gate: float32 [16, 2048], P('tp', 'sp'), may hold values from -1 to 24
- head_gain: float32 [2048], P('tp'), may hold values from 0.1 to 1.9
- out_weight: bfloat16 [2048, 2048], P('tp'), may hold values from -0.125 to 0.125
- stream: bfloat16 [2048, 2048], P('sp'), may hold values from -6 to 6
- mix_gain: float32 [2048], replicated, may hold values from 0.1 to 1.9
- up_weight: bfloat16 [2048, 8192], P('sp', 'tp'), may hold values from -0.125 to 0.125
- down_weight: bfloat16 [8192, 2048], P('tp', 'sp'), may hold values from -0.0625 to 0.0625
- out_gain: float32 [2048], replicated, may hold values from 0.1 to 1.9
Outputs:
- result: bfloat16 [2048, 2048], P(('sp', 'tp'))
All inputs are finite; a program needn't handle non-finite values.
Results may differ from a plain program's by a relative error of at most 0.018.
Values may be sent and summed in bfloat16 or wider, within the bound.
A program may use at most 128 MiB of HBM per device.

v0:
```python
from functools import partial

import jax
import jax.numpy as jnp
from jax import lax
from jax.sharding import PartitionSpec as P

BLOCK = 64


NEG_BIG = -1e30
EPS = 1e-05


def prefix_2(part, axis, combine, identity):
    place = lax.axis_index(axis)
    gathered = jax.tree.map(lambda a: lax.all_gather(a, axis), part)
    state = jax.tree.map(lambda a, e: jnp.zeros_like(a) + jnp.asarray(e, a.dtype), part, identity)

    def one(lap, state):
        return combine(
            state, jax.tree.map(lambda a: lax.dynamic_index_in_dim(a, lap, 0, False), gathered)
        )

    return lax.fori_loop(0, place, one, state)


def combine(earlier, later):
    decay_early, cell_early, norm_early, peak_early = earlier
    decay_late, cell_late, norm_late, peak_late = later
    ceiling = jnp.maximum(decay_late + peak_early, peak_late)
    keep_share = jnp.exp(decay_late + peak_early - ceiling)
    fresh_share = jnp.exp(peak_late - ceiling)
    cell_new = keep_share[..., None, None] * cell_early + fresh_share[..., None, None] * cell_late
    norm_new = keep_share[..., None] * norm_early + fresh_share[..., None] * norm_late
    return (decay_early + decay_late, cell_new, norm_new, ceiling)


def combine_groups(earlier, later):
    return (combine(earlier[0], later[0]), combine(earlier[1], later[1]))


def summarize(queries, keys_in, values_in, in_pre, forget_pre, block_len):
    length, width_k = queries.shape
    block_count = length // block_len
    scaled_keys = keys_in.astype(jnp.float32).reshape(
        block_count, block_len, width_k
    ) * width_k ** (-0.5)
    values_f = values_in.astype(jnp.float32).reshape(block_count, block_len, -1)
    width_v = values_f.shape[-1]
    log_forget = jax.nn.log_sigmoid(forget_pre).reshape(block_count, block_len)
    log_input = in_pre.reshape(block_count, block_len)
    cumulative = jnp.cumsum(log_forget, 1)
    decay_total = cumulative[:, -1]
    weight_log = decay_total[:, None] - cumulative + log_input
    peak_log = jnp.max(weight_log, 1)
    weighted = jnp.exp(weight_log - peak_log[:, None])[..., None] * scaled_keys
    cell_states = jnp.einsum("cld,cle->cde", weighted, values_f, precision=lax.Precision.HIGHEST)
    norm_states = jnp.sum(weighted, 1)
    identity = (
        jnp.zeros((), jnp.float32),
        jnp.zeros((width_k, width_v), jnp.float32),
        jnp.zeros((width_k,), jnp.float32),
        jnp.full((), NEG_BIG, jnp.float32),
    )

    def advance(running, element):
        return (combine(running, element), running)

    closing, prefix = lax.scan(advance, identity, (decay_total, cell_states, norm_states, peak_log))
    return (closing, prefix, (scaled_keys, values_f, cumulative, log_input))


def finish(queries, prefix, pieces, incoming):
    scaled_keys, values_f, cumulative, log_input = pieces
    block_count, block_len, width_k = scaled_keys.shape
    spread_in = jax.tree.map(
        lambda leaf: jnp.broadcast_to(leaf, (block_count,) + leaf.shape), incoming
    )
    _, cell_states, norm_states, peaks = combine(spread_in, prefix)
    query_f = queries.astype(jnp.float32).reshape(block_count, block_len, width_k)
    log_gaps = cumulative[:, :, None] - cumulative[:, None, :] + log_input[:, None, :]
    causal = jnp.arange(block_len)[:, None] >= jnp.arange(block_len)[None, :]
    log_gaps = jnp.where(causal[None], log_gaps, -jnp.inf)
    carried = cumulative + peaks[:, None]
    ceiling = jnp.maximum(carried, jnp.max(log_gaps, 2))
    scores = jnp.einsum("cld,csd->cls", query_f, scaled_keys, precision=lax.Precision.HIGHEST)
    scores = scores * jnp.exp(log_gaps - ceiling[..., None])
    carry_weight = jnp.exp(carried - ceiling)
    numerator = carry_weight[..., None] * jnp.einsum(
        "cld,cde->cle", query_f, cell_states, precision=lax.Precision.HIGHEST
    )
    numerator = numerator + jnp.einsum(
        "cls,cse->cle", scores, values_f, precision=lax.Precision.HIGHEST
    )
    denominator = carry_weight * jnp.einsum(
        "cld,cd->cl", query_f, norm_states, precision=lax.Precision.HIGHEST
    )
    denominator = denominator + jnp.sum(scores, 2)
    result = numerator / jnp.maximum(jnp.abs(denominator), jnp.exp(-ceiling))[..., None]
    return result.reshape(block_count * block_len, -1)


def head_norm(cell_out):
    center = jnp.mean(cell_out, -1, keepdims=True)
    spread = jnp.mean(jnp.square(cell_out - center), -1, keepdims=True)
    return (cell_out - center) * lax.rsqrt(spread + EPS)


def layer_norm(rows_f, gain):
    center = jnp.mean(rows_f, -1, keepdims=True)
    spread = jnp.mean(jnp.square(rows_f - center), -1, keepdims=True)
    return (rows_f - center) * lax.rsqrt(spread + EPS) * gain


def empty_state(head_pairs, width_k, width_v):
    return (
        jnp.zeros((head_pairs,), jnp.float32),
        jnp.zeros((head_pairs, width_k, width_v), jnp.float32),
        jnp.zeros((head_pairs, width_k), jnp.float32),
        jnp.full((head_pairs,), NEG_BIG, jnp.float32),
    )


def body(
    query_one,
    key_one,
    query_two,
    key_two,
    values,
    out_gate,
    in_gate,
    forget_gate,
    head_gain,
    out_weight,
    stream,
    mix_gain,
    up_weight,
    down_weight,
    out_gain,
):
    length = stream.shape[0]
    head_pairs = in_gate.shape[0] // 2
    width_v = values.shape[1] // (2 * head_pairs)

    def split_heads(array):
        return array.reshape(length, head_pairs, -1).transpose(1, 0, 2)

    values_split = values.reshape(length, head_pairs, 2, width_v).transpose(1, 2, 0, 3)
    input_rows = in_gate.reshape(head_pairs, 2, length)
    forget_rows = forget_gate.reshape(head_pairs, 2, length)
    summary = jax.vmap(partial(summarize, block_len=BLOCK))
    queries_one = split_heads(query_one)
    queries_two = split_heads(query_two)
    closing_one, prefix_one, pieces_one = summary(
        queries_one, split_heads(key_one), values_split[:, 0], input_rows[:, 0], forget_rows[:, 0]
    )
    closing_two, prefix_two, pieces_two = summary(
        queries_two, split_heads(key_two), values_split[:, 1], input_rows[:, 1], forget_rows[:, 1]
    )
    identity = (
        empty_state(head_pairs, queries_one.shape[2], width_v),
        empty_state(head_pairs, queries_two.shape[2], width_v),
    )
    incoming = prefix_2((closing_one, closing_two), "sp", combine_groups, identity)
    cell_one = jax.vmap(finish)(queries_one, prefix_one, pieces_one, incoming[0])
    cell_two = jax.vmap(finish)(queries_two, prefix_two, pieces_two, incoming[1])
    normed = jnp.stack([head_norm(cell_one), head_norm(cell_two)], 1)
    normed = normed.transpose(2, 0, 1, 3).reshape(length, 2 * head_pairs * width_v)
    mixed_heads = (normed * head_gain * jax.nn.sigmoid(out_gate.astype(jnp.float32))).astype(
        jnp.bfloat16
    )
    own_rows = length // lax.axis_size("tp")
    leading = lax.axis_index("tp") * own_rows
    up_full, down_full = (
        lax.all_gather(up_weight, "sp", axis=0, tiled=True),
        lax.all_gather(down_weight, "sp", axis=1, tiled=True),
    )
    summed = lax.psum_scatter(
        jnp.dot(mixed_heads, out_weight, preferred_element_type=jnp.float32).astype(jnp.bfloat16),
        "tp",
        scatter_dimension=0,
        tiled=True,
    )
    mixer_out = lax.optimization_barrier(summed)
    stream_own = lax.dynamic_slice_in_dim(stream, leading, own_rows, 0)
    first_own = layer_norm(
        stream_own.astype(jnp.float32) + mixer_out.astype(jnp.float32), mix_gain
    ).astype(jnp.bfloat16)
    hidden = jnp.square(
        jax.nn.relu(
            jnp.dot(
                lax.all_gather(first_own, "tp", axis=0, tiled=True),
                up_full,
                preferred_element_type=jnp.float32,
            )
        )
    ).astype(jnp.bfloat16)
    partial_sums = jnp.dot(hidden, down_full, preferred_element_type=jnp.float32)
    mlp_out = lax.optimization_barrier(
        lax.psum_scatter(partial_sums.astype(jnp.bfloat16), "tp", scatter_dimension=0, tiled=True)
    )
    return layer_norm(first_own.astype(jnp.float32) + mlp_out.astype(jnp.float32), out_gain).astype(
        jnp.bfloat16
    )


def solution(mesh):
    in_specs = (
        P("sp", "tp"),
        P("sp", "tp"),
        P("sp", "tp"),
        P("sp", "tp"),
        P("sp", "tp"),
        P("sp", "tp"),
        P("tp", "sp"),
        P("tp", "sp"),
        P("tp"),
        P("tp", None),
        P("sp", None),
        P(),
        P("sp", "tp"),
        P("tp", "sp"),
        P(),
    )
    out_specs = P(("sp", "tp"), None)
    return jax.shard_map(body, mesh=mesh, in_specs=in_specs, out_specs=out_specs, check_vma=False)
```

profile of v0, /device:TPU:0, one launch (start us, length us, event | category | flops | bytes accessed | tf_op | source)
XLA Modules:
  0.0 683.7 jit_solution(4655088481596444945)
XLA Ops:
  6.6 0.8 fusion.72
  7.5 1.0 reduce_window_sum.18
  8.7 0.8 fusion.88
  9.8 1.1 reshape.275
  11.0 1.0 copy.76
  12.7 0.7 while.76
  13.4 0.6 copy-done.1
  14.2 1.0 reduce_window_sum.17
  16.2 0.7 convolution_bitcast_fusion
  16.9 0.8 while.75
  17.7 0.7 copy-done
  18.6 0.6 dynamic-slice
  20.6 43.8 %all-reduce.4 = (f32[64]{0:T(128)S(1)}, f32[64]{0:T(128)S(1)}, f32[64]{0:T(128)S(1)}, f32[64]{0:T(128)S(1)}) all-reduce(f32[64]{0:T(128)S(1)} %dynamic-update-slice, f32[64]{0:T(128)S(1)} %dynamic-update-slice.1, f32[64]{0:T(128)S(1)} %dynamic-update-slice.2, f32[64]{0:T(128)S(1)} %dynamic-update-slice.3), channel_id=2, replica_groups=mesh['sp'=16,'tp'=2] {'sp'}, use_global_device_ids=true, to_apply=%add | all-reduce | flops 256 | bytes 2048
  65.1 36.1 %all-gather.9 = f32[16,4,64]{2,1,0:T(4,128)S(1)} all-gather(f32[1,4,64]{2,1,0:T(4,128)S(1)} %bitcast.311), channel_id=9, replica_groups=mesh['sp'=16,'tp'=2] {'sp'}, dimensions={0}, use_global_device_ids=true | all-gather | bytes 17408 | tf_op jit(solution)/shard_map/all_gather | solution.py:17
  101.3 37.9 %all-gather.8 = f32[16,4,128]{2,1,0:T(4,128)S(1)} all-gather(f32[1,4,128]{2,1,0:T(4,128)S(1)} %bitcast.312), channel_id=5, replica_groups=mesh['sp'=16,'tp'=2] {'sp'}, dimensions={0}, use_global_device_ids=true | all-gather | bytes 34816 | tf_op jit(solution)/shard_map/all_gather | solution.py:17
  139.6 15.4 %all-gather.19.cloned.1.call-done = f32[64,128,128]{2,1,0:T(8,128)} async-done(((f32[4,128,128]{2,1,0:T(8,128)}), f32[64,128,128]{2,1,0:T(8,128)}) %all-gather.19.cloned.1.call-update) | async-done | bytes 4194320 | tf_op jit(solution)/shard_map/all_gather | solution.py:17
  156.7 0.5 fusion.92
  161.0 3.8 convolution_convert_fusion.1
  164.9 0.5 all-gather.15.cloned.1.call-update
  165.5 0.5 all-gather.17.cloned.1.call-update
  166.1 39.8 %reduce-scatter.3.cloned.1.call-done = bf16[64,2048]{1,0:T(8,128)(2,1)} async-done(((bf16[128,2048]{1,0:T(8,128)(2,1)}), bf16[64,2048]{1,0:T(8,128)(2,1)}) %reduce-scatter.3.cloned.1.call-update) | async-done | bytes 262160 | tf_op jit(solution)/shard_map/reduce_scatter | solution.py:179
  206.0 1.1 fusion.39
  207.1 1.2 multiply_reduce_fusion.1
  208.3 1.1 multiply_convert_fusion.1
  209.4 2.4 all_gather.73
  211.8 189.0 %all-gather.15.cloned.1.call-done = bf16[2048,4096]{1,0:T(8,128)(2,1)} async-done(((bf16[128,4096]{1,0:T(8,128)(2,1)}), bf16[2048,4096]{1,0:T(8,128)(2,1)}) %all-gather.15.cloned.1.call-update) | async-done | bytes 16777232 | tf_op jit(solution)/shard_map/all_gather | solution.py:176
  400.7 249.9 %all-gather.17.cloned.1.call-done = bf16[4096,2048]{1,0:T(8,128)(2,1)} async-done(((bf16[4096,128]{1,0:T(8,128)(2,1)}), bf16[4096,2048]{1,0:T(8,128)(2,1)}) %all-gather.17.cloned.1.call-update) | async-done | bytes 16777232 | tf_op jit(solution)/shard_map/all_gather | solution.py:177
  650.6 15.9 %convolution_convert_fusion = bf16[128,2048]{1,0:T(8,128)(2,1)} fusion(bf16[4096,2048]{1,0:T(8,128)(2,1)} %all-gather.17.cloned.1.call-done, bf16[128,2048]{1,0:T(8,128)(2,1)S(1)} %all_gather.73, bf16[2048,4096]{1,0:T(8,128)(2,1)} %all-gather.15.cloned.1.call-done), kind=kOutput, calls=%fused_computation.65 | convolution fusion | flops 4296802304 | bytes 34603008 | tf_op jit(solution)/shard_map/dot_general | solution.py:199
  666.5 6.3 reduce-scatter.5.cloned.1.call-done
  672.8 1.1 fusion.41
  673.9 1.2 multiply_reduce_fusion
  675.1 1.8 multiply_convert_fusion
  (173 shorter events, 11.5 us)
Async XLA Ops:
  6.5 9.0 %copy-start.3 = (bf16[128,512]{1,0:T(8,128)(2,1)S(1)}, bf16[128,512]{1,0:T(8,128)(2,1)}, u32[]{:S(2)}) copy-start(bf16[128,512]{1,0:T(8,128)(2,1)} %param.22) | copy-start | bytes 393220
  6.5 133.0 %all-gather.21.cloned.1.call-start = ((), (), s32[]{:S(2)}) async-start(), calls=%async_computation.7 | async-start | bytes 2228224 | tf_op jit(solution)/shard_map/all_gather | solution.py:17
  13.4 0.6 copy-start.1
  14.0 140.9 %all-gather.19.cloned.1.call-start = ((), (), s32[]{:S(2)}) async-start(), calls=%async_computation.6 | async-start | bytes 4456448 | tf_op jit(solution)/shard_map/all_gather | solution.py:17
  16.2 2.4 copy-start.10
  16.2 48.6 %copy-start.4 = (bf16[128,512]{1,0:T(8,128)(2,1)S(1)}, bf16[128,512]{1,0:T(8,128)(2,1)}, u32[]{:S(2)}) copy-start(bf16[128,512]{1,0:T(8,128)(2,1)} %param.21) | copy-start | bytes 393220
  16.9 48.0 %copy-start.5 = (bf16[128,256]{1,0:T(8,128)(2,1)S(1)}, bf16[128,256]{1,0:T(8,128)(2,1)}, u32[]{:S(2)}) copy-start(bf16[128,256]{1,0:T(8,128)(2,1)} %param.23) | copy-start | bytes 196612
  17.7 0.7 copy-start
  18.4 187.6 %reduce-scatter.3.cloned.1.call-start = ((), (), s32[]{:S(2)}) async-start(), calls=%async_computation.2 | async-start | bytes 786432 | tf_op jit(solution)/shard_map/reduce_scatter | solution.py:179
  157.2 3.8 copy-start.8
  157.2 3.8 copy-start.9
  161.0 44.9 %copy-start.2 = (bf16[128,2048]{1,0:T(8,128)(2,1)S(1)}, bf16[128,2048]{1,0:T(8,128)(2,1)}, u32[]{:S(2)}) copy-start(bf16[128,2048]{1,0:T(8,128)(2,1)} %param.31) | copy-start | bytes 1572868
  161.0 47.3 %copy-start.6 = (f32[2048]{0:T(1024)S(1)}, f32[2048]{0:T(1024)}, u32[]{:S(2)}) copy-start(f32[2048]{0:T(1024)} %param.32) | copy-start | bytes 24580
  164.9 235.8 %all-gather.15.cloned.1.call-start = ((), (), s32[]{:S(2)}) async-start(), calls=%async_computation.3 | async-start | bytes 17825792 | tf_op jit(solution)/shard_map/all_gather | solution.py:176
  165.5 485.1 %all-gather.17.cloned.1.call-start = ((), (), s32[]{:S(2)}) async-start(), calls=%async_computation.4 | async-start | bytes 17825792 | tf_op jit(solution)/shard_map/all_gather | solution.py:177
  166.1 506.7 %reduce-scatter.5.cloned.1.call-start = ((), (), s32[]{:S(2)}) async-start(), calls=%async_computation.5 | async-start | bytes 786432 | tf_op jit(solution)/shard_map/reduce_scatter | solution.py:201
  211.8 463.3 %copy-start.7 = (f32[2048]{0:T(1024)S(1)}, f32[2048]{0:T(1024)}, u32[]{:S(2)}) copy-start(f32[2048]{0:T(1024)} %param.35) | copy-start | bytes 24580
Sparse Core Ops, SparseCore 0:
  14.2 63.5 all-gather.20
  80.5 74.4 all-gather.18
  165.0 40.8 reduce-scatter.2
  208.6 192.1 all-gather.14
  403.3 247.2 all-gather.16
  666.6 6.0 reduce-scatter.4
where the time goes:
time: 685 us; the launch traced here: 684 us
  waiting for transfers between devices  501 us (73%)
  blocking collectives  120 us (18%)
  matrix products  23.7 us (3%)
  between operations  14.6 us (2%)
  other arithmetic  13.8 us (2%)
  local copies, waits for them, and re-layouts  9.5 us (1%)
    all_gather x1, waiting for transfers between devices, body(): lax.all_gather(down_weight, 'sp', axis=1, tiled=True)  250 us
    all_gather x1, waiting for transfers between devices, body(): lax.all_gather(up_weight, 'sp', axis=0, tiled=True)  189 us
    all_gather x2, blocking collectives, prefix_2(): gathered = jax.tree.map(lambda a: lax.all_gather(a, axis), part)  74.1 us
    unnamed x1, blocking collectives  43.8 us
    reduce_scatter x1, waiting for transfers between devices, body(): lax.psum_scatter(jnp.dot(mixed_heads, out_weight, preferred_element_type=...  39.8 us
    dot_general x1, matrix products, body(): jnp.dot(hidden, down_full, preferred_element_type=jnp.float32)  15.9 us
    all_gather x2, waiting for transfers between devices, prefix_2(): gathered = jax.tree.map(lambda a: lax.all_gather(a, axis), part)  15.4 us
  transfers between devices with their start and end apart: 6, of which 5 were waited for; matrix products, arithmetic and copies ran while one was open for 1% of the time, Pallas kernels for 0%

commit v1 on v0

v1 whole, which is shorter than its diff:
```python
import functools

import jax
import jax.numpy as jnp
from jax import lax
from jax.experimental import pallas as pl
from jax.experimental.pallas import tpu as pltpu
from jax.sharding import PartitionSpec as P

NEG_BIG = -1e30
EPS = 1e-05
F32 = jnp.float32
BF16 = jnp.bfloat16
MESH_ID = pl.DeviceIdType.MESH


def dot(a, b):
    return jnp.dot(a, b, preferred_element_type=F32)


def halves(a):
    high = a.astype(BF16)
    return high, (a - high.astype(F32)).astype(BF16)


def dot_left(a, b):
    high, low = halves(a)
    return dot(high, b) + dot(low, b)


def dot_right(a, b):
    high, low = halves(b)
    return dot(a, high) + dot(a, low)


def layer_norm(rows_f, gain):
    center = jnp.mean(rows_f, -1, keepdims=True)
    spread = jnp.mean(jnp.square(rows_f - center), -1, keepdims=True)
    return (rows_f - center) * lax.rsqrt(spread + EPS) * gain


def kernel(
    ns, ntp, nt, early,
    q1, k1, q2, k2, v, og, ig, fg, hg, ow, stream, mg, up, down, outg,
    out,
    up_slab, dn_slab, ow_v, state, sh_in, sh_out, c_in, small, small_all, peaks, norms,
    mixed, part, mix_in, xg, pbuf, tp_in, rs_out, rs_in,
    own_sem, up_s, up_r, dn_s, dn_r, st_s, st_r, sm_s, sm_r, ci_s, ci_r, mx_s, mx_r,
    ag_s, ag_r, fw_s, tp_s, tp_r, rs_s, rs_r,
):
    s = lax.axis_index("sp")
    c = lax.axis_index("tp")
    nw = ns // nt
    w, t = s // nt, lax.rem(s, nt)
    length = q1.shape[0]
    gates = ig.shape[0]
    pairs = gates // 2
    ka, kb = q1.shape[1] // pairs, q2.shape[1] // pairs
    dv = v.shape[1] // gates
    depth = up.shape[0]
    width = up_slab.shape[1]
    own = out.shape[0]
    shard = sh_in.shape[1]

    def remote(src, dst, send, recv, sp, tp):
        return pltpu.make_async_remote_copy(
            src_ref=src, dst_ref=dst, send_sem=send, recv_sem=recv,
            device_id=(sp, tp), device_id_type=MESH_ID,
        )

    def loop(low, high, fn):
        def step(i, carry):
            fn(i)
            return carry

        lax.fori_loop(low, high, step, 0)

    def peer(j):
        return lax.rem(s + j, ns)

    def mate(j):
        return lax.rem(c + j, ntp)

    barrier = pltpu.get_barrier_semaphore()
    loop(1, ns, lambda j: pl.semaphore_signal(
        barrier, inc=1, device_id=(peer(j), c), device_id_type=MESH_ID))
    loop(1, ntp, lambda j: pl.semaphore_signal(
        barrier, inc=1, device_id=(s, mate(j)), device_id_type=MESH_ID))

    def up_part(which):
        return up.at[:, pl.ds(pl.multiple_of(which * width, 128), width)]

    def dn_part(which):
        return down.at[pl.ds(pl.multiple_of(which * width, 128), width), :]

    def up_rows(source):
        return up_slab.at[pl.ds(pl.multiple_of(source * depth, depth), depth), :]

    own_up = pltpu.make_async_copy(up_part(w), up_rows(s), own_sem.at[0])
    own_dn = pltpu.make_async_copy(dn_part(w), dn_slab.at[s], own_sem.at[1])
    own_ow = pltpu.make_async_copy(ow, ow_v, own_sem.at[2])
    own_ow.start()
    own_up.start()
    own_dn.start()

    def up_copy(j):
        to = peer(j)
        return remote(up_part(to // nt), up_rows(s), up_s.at[j], up_r.at[s], to, c)

    def dn_copy(j):
        to = peer(j)
        return remote(dn_part(to // nt), dn_slab.at[s], dn_s.at[j], dn_r.at[s], to, c)

    pl.semaphore_wait(barrier, ns - 1 + ntp - 1)
    loop(1, early, lambda j: up_copy(j).start())

    forget = fg[...]
    log_forget = jnp.minimum(forget, 0.0) - jnp.log1p(jnp.exp(-jnp.abs(forget)))
    row_id = lax.broadcasted_iota(jnp.int32, (length, length), 0)
    col_id = lax.broadcasted_iota(jnp.int32, (length, length), 1)
    causal = row_id >= col_id
    upper = (row_id <= col_id).astype(F32)
    eye = (row_id == col_id).astype(F32)
    exact = lax.Precision.HIGHEST
    cumulative = jnp.dot(log_forget, upper, precision=exact, preferred_element_type=F32)
    log_input = ig[...]
    total = cumulative[:, length - 1:length]
    weight_log = total - cumulative + log_input
    peak = jnp.max(weight_log, 1, keepdims=True)
    weight = jnp.exp(weight_log - peak)
    key_t1 = jnp.transpose(k1[...].astype(F32))
    key_t2 = jnp.transpose(k2[...].astype(F32))
    norm_1 = dot_left(weight, k1[...]) * ka ** -0.5
    norm_2 = dot_left(weight, k2[...]) * kb ** -0.5
    norm_rows = []
    used = pairs * (ka + kb)
    if used < state.shape[0]:
        state[used:, :] = jnp.zeros((state.shape[0] - used, dv), F32)
    heads = []
    for g in range(gates):
        j, two = g // 2, g % 2
        size = kb if two else ka
        base = pairs * ka * two + j * size
        key_t = (key_t2 if two else key_t1)[j * size:(j + 1) * size]
        query = (q2 if two else q1)[:, j * size:(j + 1) * size]
        heads.append((size, base, key_t, query))
        state[base:base + size, :] = dot_left(
            key_t * (weight[g:g + 1] * size ** -0.5), v[:, g * dv:(g + 1) * dv])
        row = (norm_2 if two else norm_1)[g:g + 1, j * size:(j + 1) * size]
        if size < ka:
            row = jnp.concatenate([row, jnp.zeros((1, ka - size), F32)], 1)
        norm_rows.append(row)
    small[0] = jnp.broadcast_to(total, (gates, ka))
    small[1] = jnp.broadcast_to(peak, (gates, ka))
    small[2] = jnp.concatenate(norm_rows, 0)

    def rows_of(which):
        return pl.ds(pl.multiple_of(which * shard, 8), shard)

    def small_copy(j):
        return remote(small, small_all.at[s], sm_s.at[j], sm_r.at[s], peer(j), c)

    def state_copy(j):
        to = peer(j)
        return remote(state.at[rows_of(to), :], sh_in.at[s], st_s.at[j], st_r.at[s], to, c)

    def first_sends(j):
        small_copy(j).start()
        state_copy(j).start()

    loop(1, ns, first_sends)
    loop(early, ns, lambda j: up_copy(j).start())
    small_all[s] = small[...]
    sh_in[s] = state[rows_of(s), :]

    def first_waits(j):
        source = peer(j)
        remote(small, small_all.at[source], sm_s.at[j], sm_r.at[source], source, c).wait_recv()
        remote(state.at[rows_of(s), :], sh_in.at[source], st_s.at[j], st_r.at[source],
               source, c).wait_recv()

    loop(1, ns, first_waits)

    shard_row = s * shard + lax.broadcasted_iota(jnp.int32, (shard, dv), 0)

    def spread(rows):
        full = jnp.zeros((shard, dv), F32)
        for g in range(gates):
            size, base = heads[g][:2]
            inside = (shard_row >= base) & (shard_row < base + size)
            full = jnp.where(inside, rows[g:g + 1, :], full)
        return full

    def advance(e, carry):
        run, peak_run, norm_run = carry
        sh_out[e] = run
        peaks[e] = peak_run
        norms[e] = norm_run
        decayed = peak_run + small_all[e, 0]
        fresh = small_all[e, 1]
        ceiling = jnp.maximum(decayed, fresh)
        keep = jnp.exp(decayed - ceiling)
        new = jnp.exp(fresh - ceiling)
        return (
            run * spread(keep) + sh_in[e] * spread(new),
            ceiling,
            norm_run * keep + small_all[e, 2] * new,
        )

    lax.fori_loop(0, ns, advance, (
        jnp.zeros((shard, dv), F32),
        jnp.full((gates, ka), NEG_BIG, F32),
        jnp.zeros((gates, ka), F32),
    ))

    def back_copy(j):
        to = peer(j)
        return remote(sh_out.at[to], c_in.at[rows_of(s), :], ci_s.at[j], ci_r.at[s], to, c)

    loop(1, ns, lambda j: back_copy(j).start())
    loop(1, ns, lambda j: dn_copy(j).start())
    c_in[rows_of(s), :] = sh_out[s]
    peak_in = peaks[s]
    norm_in = norms[s]

    cum_cols = lax.dot_general(eye, cumulative, (((1,), (1,)), ((), ())), precision=exact,
                               preferred_element_type=F32)
    column = log_input - cumulative

    def back_waits(j):
        source = peer(j)
        remote(sh_out.at[s], c_in.at[rows_of(source), :], ci_s.at[j], ci_r.at[source],
               source, c).wait_recv()

    inside = []
    for g in range(gates):
        size, base, key_t, query = heads[g]
        cum_col = cum_cols[:, g:g + 1]
        gaps = jnp.where(causal, cum_col + column[g:g + 1], NEG_BIG)
        carried = cum_col + peak_in[g:g + 1, 0:1]
        ceiling = jnp.maximum(carried, jnp.max(gaps, 1, keepdims=True))
        scores = dot(query, key_t.astype(BF16)) * size ** -0.5 * jnp.exp(gaps - ceiling)
        carry_weight = jnp.exp(carried - ceiling)
        numerator = dot_left(scores, v[:, g * dv:(g + 1) * dv])
        denominator = carry_weight * jnp.sum(
            query.astype(F32) * norm_in[g:g + 1, :size], 1, keepdims=True)
        denominator = denominator + jnp.sum(scores, 1, keepdims=True)
        bound = jnp.maximum(jnp.abs(denominator), jnp.exp(-ceiling))
        inside.append((numerator, carry_weight, bound))
    loop(1, ns, back_waits)
    for g in range(gates):
        size, base, key_t, query = heads[g]
        numerator, carry_weight, bound = inside[g]
        cell = (numerator + carry_weight * dot_right(query, c_in[base:base + size, :])) / bound
        center = jnp.mean(cell, -1, keepdims=True)
        variance = jnp.mean(jnp.square(cell - center), -1, keepdims=True)
        cols = slice(g * dv, (g + 1) * dv)
        gate = jax.nn.sigmoid(og[:, cols].astype(F32))
        mixed[:, cols] = (
            (cell - center) * lax.rsqrt(variance + EPS) * hg[:, cols] * gate).astype(BF16)

    own_ow.wait()
    for p in range(0, ow.shape[1], 512):
        part[:, p:p + 512] = dot(mixed[...], ow_v[:, p:p + 512]).astype(BF16)

    def own_block(which):
        return pl.ds(pl.multiple_of(which * own, own), own)

    def mix_copy(j):
        to = mate(j)
        return remote(part.at[own_block(to), :], mix_in.at[c], mx_s.at[j], mx_r.at[c], s, to)

    loop(1, ntp, lambda j: mix_copy(j).start())
    mix_in[c] = part[own_block(c), :]
    for j in range(1, ntp):
        source = mate(j)
        remote(part.at[own_block(c), :], mix_in.at[source], mx_s.at[j], mx_r.at[source],
               s, source).wait_recv()
    mixer = mix_in[0].astype(F32)
    for j in range(1, ntp):
        mixer = mixer + mix_in[j].astype(F32)
    mixer = mixer.astype(BF16).astype(F32)
    first = layer_norm(stream[own_block(c), :].astype(F32) + mixer, mg[...]).astype(BF16)
    xg[w * ntp + c] = first

    def group(j):
        return lax.rem(w + j, nw)

    def share_copy(j):
        slot = w * ntp + c
        return remote(xg.at[slot], xg.at[slot], ag_s.at[j], ag_r.at[slot], group(j) * nt + t, c)

    def hand_copy(from_w, j):
        slot = from_w * ntp + c
        return remote(xg.at[slot], xg.at[slot], fw_s.at[from_w * ntp + j], ag_r.at[slot],
                      s, mate(j))

    loop(1, nw, lambda j: share_copy(j).start())
    loop(1, ntp, lambda j: hand_copy(w, j).start())

    def slot_wait(slot):
        remote(xg.at[slot], xg.at[slot], ag_s.at[0], ag_r.at[slot], s, c).wait_recv()

    own_up.wait()
    own_dn.wait()

    def weight_waits(j):
        source = peer(j)
        remote(up_part(w), up_rows(source), up_s.at[j], up_r.at[source], source, c).wait_recv()
        remote(dn_part(w), dn_slab.at[source], dn_s.at[j], dn_r.at[source], source, c).wait_recv()

    joined = max(1, 256 // depth)

    def arrive(j):
        from_w = group(nw - j)
        slot_wait(from_w * ntp + c)
        loop(1, ntp, lambda i: hand_copy(from_w, i).start())

    def tp_copy(to_w, j):
        to = mate(j)
        return remote(pbuf.at[to_w, own_block(to), :], tp_in.at[to_w, c],
                      tp_s.at[to_w * ntp + j], tp_r.at[to_w * ntp + c], s, to)

    def mixer_step(j):
        from_w = group(nw - j)
        loop(1, ntp, lambda i: slot_wait(from_w * ntp + mate(i)))
        rows = xg[pl.ds(from_w * ntp, ntp)].reshape(ntp * own, xg.shape[2])
        hidden = jnp.square(jnp.maximum(dot(rows, up_slab[...]), 0.0)).astype(BF16)
        for a in range(0, ns, joined):
            block = jnp.concatenate([dn_slab[a + i] for i in range(joined)], 1)
            pbuf[from_w, :, a * depth:(a + joined) * depth] = dot(hidden, block).astype(BF16)
        loop(1, ntp, lambda i: tp_copy(from_w, i).start())

    def sum_copy(to_w, j):
        return remote(rs_out.at[to_w], rs_in.at[w], rs_s.at[j], rs_r.at[w], to_w * nt + t, c)

    def pair_sum(j):
        to_w = group(nw - j)
        for i in range(1, ntp):
            source = mate(i)
            remote(pbuf.at[to_w, own_block(c), :], tp_in.at[to_w, source],
                   tp_s.at[to_w * ntp + i], tp_r.at[to_w * ntp + source], s, source).wait_recv()
        added = pbuf[to_w, own_block(c), :].astype(F32)
        for i in range(1, ntp):
            added = added + tp_in[to_w, mate(i)].astype(F32)
        return to_w, added.astype(BF16)

    def send_sum(j):
        to_w, added = pair_sum(j)
        rs_out[to_w] = added
        sum_copy(to_w, j).start()

    loop(1, ns, weight_waits)
    arrive(1)

    def step(j, carry):
        @pl.when(j < nw - 1)
        def _():
            arrive(j + 1)

        mixer_step(j)

        @pl.when(j > 1)
        def _():
            send_sum(j - 1)

        return carry

    lax.fori_loop(1, nw, step, 0)
    mixer_step(nw)
    send_sum(nw - 1)
    _, added = pair_sum(nw)
    rs_in[w] = added

    def sum_wait(j):
        source = group(j)
        remote(rs_out.at[source], rs_in.at[source], rs_s.at[j], rs_r.at[source],
               source * nt + t, c).wait_recv()

    loop(1, nw, sum_wait)
    mlp_out = rs_in[0].astype(F32)
    for i in range(1, nw):
        mlp_out = mlp_out + rs_in[i].astype(F32)
    mlp_out = mlp_out.astype(BF16).astype(F32)
    out[...] = layer_norm(xg[w * ntp + c].astype(F32) + mlp_out, outg[...]).astype(BF16)

    def drain(j):
        up_copy(j).wait_send()
        dn_copy(j).wait_send()
        small_copy(j).wait_send()
        state_copy(j).wait_send()
        back_copy(j).wait_send()

    loop(1, ns, drain)
    loop(1, ntp, lambda j: mix_copy(j).wait_send())

    def drain_group(j):
        share_copy(j).wait_send()
        sum_copy(group(nw - j), j).wait_send()

    loop(1, nw, drain_group)

    def drain_pair(a):
        for j in range(1, ntp):
            hand_copy(a, j).wait_send()
            tp_copy(a, j).wait_send()

    loop(0, nw, drain_pair)


def body(mesh, *args):
    (q1, k1, q2, k2, v, og, ig, fg, hg, ow, stream, mg, up, down, outg) = args
    ns, ntp = mesh.shape["sp"], mesh.shape["tp"]
    nt = 2
    while (up.shape[1] // (ns // nt)) % 128:
        nt *= 2
    nw = ns // nt
    width = up.shape[1] // nw
    depth = up.shape[0]
    length, model = stream.shape
    own = length // ntp
    gates = ig.shape[0]
    dv = v.shape[1] // gates
    ka = 2 * q1.shape[1] // gates
    used = q1.shape[1] + q2.shape[1]
    shard = -(-used // (ns * 8)) * 8
    vm = pl.BlockSpec(memory_space=pltpu.VMEM)
    hbm = pl.BlockSpec(memory_space=pl.ANY)
    sem = pltpu.SemaphoreType.DMA
    return pl.pallas_call(
        functools.partial(kernel, ns, ntp, nt, ns // 2),
        out_shape=jax.ShapeDtypeStruct((own, model), BF16),
        in_specs=[vm] * 9 + [hbm, vm, vm, hbm, hbm, vm],
        out_specs=vm,
        scratch_shapes=[
            pltpu.VMEM((model, width), BF16),
            pltpu.VMEM((ns, width, depth), BF16),
            pltpu.VMEM(ow.shape, BF16),
            pltpu.VMEM((ns * shard, dv), F32),
            pltpu.VMEM((ns, shard, dv), F32),
            pltpu.VMEM((ns, shard, dv), F32),
            pltpu.VMEM((ns * shard, dv), F32),
            pltpu.VMEM((3, gates, ka), F32),
            pltpu.VMEM((ns, 3, gates, ka), F32),
            pltpu.VMEM((ns, gates, ka), F32),
            pltpu.VMEM((ns, gates, ka), F32),
            pltpu.VMEM((length, v.shape[1]), BF16),
            pltpu.VMEM((length, model), BF16),
            pltpu.VMEM((ntp, own, model), BF16),
            pltpu.VMEM((nw * ntp, own, model), BF16),
            pltpu.VMEM((nw, length, model), BF16),
            pltpu.VMEM((nw, ntp, own, model), BF16),
            pltpu.VMEM((nw, own, model), BF16),
            pltpu.VMEM((nw, own, model), BF16),
            sem((3,)),
        ] + [sem((ns,))] * 10 + [sem((ntp,))] * 2 + [
            sem((nw,)), sem((nw * ntp,)), sem((nw * ntp,)), sem((nw * ntp,)),
            sem((nw * ntp,)), sem((nw,)), sem((nw,)),
        ],
        compiler_params=pltpu.CompilerParams(
            collective_id=0, has_side_effects=True, vmem_limit_bytes=60 * 1024 * 1024),
    )(q1, k1, q2, k2, v, og, ig, fg, hg.reshape(1, -1), ow, stream, mg.reshape(1, -1),
      up, down, outg.reshape(1, -1))


def solution(mesh):
    in_specs = (
        P("sp", "tp"),
        P("sp", "tp"),
        P("sp", "tp"),
        P("sp", "tp"),
        P("sp", "tp"),
        P("sp", "tp"),
        P("tp", "sp"),
        P("tp", "sp"),
        P("tp"),
        P("tp", None),
        P("sp", None),
        P(),
        P("sp", "tp"),
        P("tp", "sp"),
        P(),
    )
    out_specs = P(("sp", "tp"), None)
    return jax.shard_map(functools.partial(body, mesh), mesh=mesh, in_specs=in_specs,
                         out_specs=out_specs, check_vma=False)
```

time: 685 us -> 233 us (0.34)
  waiting for transfers between devices: 501 us -> 0 us
  Pallas kernels: 0 us -> 231 us
  blocking collectives: 120 us -> 0 us
  matrix products: 23.7 us -> 0 us
  between operations: 14.6 us -> 0.01 us
  other arithmetic: 13.8 us -> 0 us
  local copies, waits for them, and re-layouts: 9.5 us -> 1.67 us
    all_gather x4 -> x0, waiting for transfers between devices: 454 us -> none  [the longest x1 250 us: body(): lax.all_gather(down_weight, 'sp', axis=1, tiled=True)]
    pallas_call x0 -> x1, Pallas kernels: none -> 231 us  [body(): pl.pallas_call(functools.partial(kernel, ns, ntp, nt, ns // 2), out_shape...]
    all_gather x3 -> x0, blocking collectives: 76.4 us -> none  [the longest x2 74.1 us: prefix_2(): gathered = jax.tree.map(lambda a: lax.all_gather(a, axis), part)]
    reduce_scatter x2 -> x0, waiting for transfers between devices: 46.1 us -> none  [the longest x1 39.8 us: body(): lax.psum_scatter(jnp.dot(mixed_heads, out_weight, preferred_element_type=...]
    unnamed x1 -> x0, blocking collectives: 43.8 us -> none
    dot_general x12 -> x0, matrix products: 23.7 us -> none  [the longest x1 15.9 us: body(): jnp.dot(hidden, down_full, preferred_element_type=jnp.float32)]
  transfers between devices with their start and end apart: 6 -> 0, of which waited for: 5 -> 0; matrix products, arithmetic and copies ran while one was open for 1% -> 0% of each run, Pallas kernels for 0% -> 0%
where the time goes in v1:
time: 233 us
  Pallas kernels  231 us (99%)
    pallas_call x1, Pallas kernels, body(): pl.pallas_call(functools.partial(kernel, ns, ntp, nt, ns // 2), out_shape...  231 us

profile of v1, /device:TPU:0, one launch (start us, length us, event | category | flops | bytes accessed | tf_op | source)
XLA Modules:
  0.0 233.1 jit_solution(6019649997046608830)
XLA Ops:
  0.0 231.4 %shard_map.145 = bf16[64,2048]{1,0:T(8,128)(2,1)} custom-call(bf16[128,512]{1,0:T(8,128)(2,1)} %q1.1, bf16[128,512]{1,0:T(8,128)(2,1)} %k1.1, bf16[128,256]{1,0:T(8,128)(2,1)} %q2.1, bf16[128,256]{1,0:T(8,128)(2,1)} %k2.1, bf16[128,1024]{1,0:T(8,128)(2,1)} %v.1, bf16[128,1024]{1,0:T(8,128)(2,1)} %og.1, f32[8,128]{1,0:T(8,128)} %ig.1, f32[8,128]{1,0:T(8,128)} %fg.1, ...), custom_call_target="tpu_custom_call" | custom-call | tf_op jit(solution)/shard_map/pallas_call | solution.py:430
  231.4 1.7 copy.17

commit v2 on v1

--- a/solution.py
+++ b/solution.py
@@ -40,18 +40,20 @@
 
 
 def kernel(
-    ns, ntp, nt, early,
+    ns, ntp, nt, ny,
     q1, k1, q2, k2, v, og, ig, fg, hg, ow, stream, mg, up, down, outg,
     out,
     up_slab, dn_slab, ow_v, state, sh_in, sh_out, c_in, small, small_all, peaks, norms,
-    mixed, part, mix_in, xg, pbuf, tp_in, rs_out, rs_in,
-    own_sem, up_s, up_r, dn_s, dn_r, st_s, st_r, sm_s, sm_r, ci_s, ci_r, mx_s, mx_r,
-    ag_s, ag_r, fw_s, tp_s, tp_r, rs_s, rs_r,
+    mixed, part, mix_in, xg, pbuf, tp_in, y_out, y_in, rs_out, rs_in,
+    own_sem, up_f, dn_f, up_s, up_r, dn_s, dn_r, st_s, st_r, sm_s, sm_r, ci_s, ci_r, mx_s, mx_r,
+    ag_s, yf_s, yr_s, yr_r, ag_r, fw_s, tp_s, tp_r, rs_s, rs_r,
 ):
     s = lax.axis_index("sp")
     c = lax.axis_index("tp")
     nw = ns // nt
     w, t = s // nt, lax.rem(s, nt)
+    nz = nw // ny
+    z, y = w // ny, lax.rem(w, ny)
     length = q1.shape[0]
     gates = ig.shape[0]
     pairs = gates // 2
@@ -104,15 +106,40 @@
     own_dn.start()
 
     def up_copy(j):
-        to = peer(j)
-        return remote(up_part(to // nt), up_rows(s), up_s.at[j], up_r.at[s], to, c)
+        to = lax.rem(w + j, nw)
+        return remote(up_part(to), up_rows(s), up_s.at[j], up_r.at[s], to * nt + t, c)
 
     def dn_copy(j):
-        to = peer(j)
-        return remote(dn_part(to // nt), dn_slab.at[s], dn_s.at[j], dn_r.at[s], to, c)
+        to = lax.rem(w + j, nw)
+        return remote(dn_part(to), dn_slab.at[s], dn_s.at[j], dn_r.at[s], to * nt + t, c)
+
+    def up_hand(j, i):
+        source = lax.rem(w + nw - j, nw) * nt + t
+        return remote(up_rows(source), up_rows(source), up_f.at[j * nt + i],
+                      up_r.at[source], w * nt + lax.rem(t + i, nt), c)
+
+    def dn_hand(j, i):
+        source = lax.rem(w + nw - j, nw) * nt + t
+        return remote(dn_slab.at[source], dn_slab.at[source], dn_f.at[j * nt + i],
+                      dn_r.at[source], w * nt + lax.rem(t + i, nt), c)
+
+    def up_wait(source):
+        remote(up_part(w), up_rows(source), up_s.at[0], up_r.at[source], peer(1), c).wait_recv()
+
+    def dn_wait(source):
+        remote(dn_part(w), dn_slab.at[source], dn_s.at[0], dn_r.at[source], peer(1),
+               c).wait_recv()
+
+    def up_pass(j):
+        up_wait(lax.rem(w + nw - j, nw) * nt + t)
+        loop(1, nt, lambda i: up_hand(j, i).start())
+
+    def dn_pass(j):
+        dn_wait(lax.rem(w + nw - j, nw) * nt + t)
+        loop(1, nt, lambda i: dn_hand(j, i).start())
 
     pl.semaphore_wait(barrier, ns - 1 + ntp - 1)
-    loop(1, early, lambda j: up_copy(j).start())
+    loop(1, nw // 2, lambda j: up_copy(j).start())
 
     forget = fg[...]
     log_forget = jnp.minimum(forget, 0.0) - jnp.log1p(jnp.exp(-jnp.abs(forget)))
@@ -169,7 +196,7 @@
         state_copy(j).start()
 
     loop(1, ns, first_sends)
-    loop(early, ns, lambda j: up_copy(j).start())
+    loop(nw // 2, nw, lambda j: up_copy(j).start())
     small_all[s] = small[...]
     sh_in[s] = state[rows_of(s), :]
 
@@ -218,7 +245,10 @@
         return remote(sh_out.at[to], c_in.at[rows_of(s), :], ci_s.at[j], ci_r.at[s], to, c)
 
     loop(1, ns, lambda j: back_copy(j).start())
-    loop(1, ns, lambda j: dn_copy(j).start())
+    loop(1, nw, lambda j: dn_copy(j).start())
+    own_up.wait()
+    loop(1, nt, lambda i: up_hand(0, i).start())
+    loop(1, nw, up_pass)
     c_in[rows_of(s), :] = sh_out[s]
     peak_in = peaks[s]
     norm_in = norms[s]
@@ -283,46 +313,61 @@
     first = layer_norm(stream[own_block(c), :].astype(F32) + mixer, mg[...]).astype(BF16)
     xg[w * ntp + c] = first
 
-    def group(j):
-        return lax.rem(w + j, nw)
-
-    def share_copy(j):
-        slot = w * ntp + c
-        return remote(xg.at[slot], xg.at[slot], ag_s.at[j], ag_r.at[slot], group(j) * nt + t, c)
-
     def hand_copy(from_w, j):
         slot = from_w * ntp + c
         return remote(xg.at[slot], xg.at[slot], fw_s.at[from_w * ntp + j], ag_r.at[slot],
                       s, mate(j))
 
-    loop(1, nw, lambda j: share_copy(j).start())
-    loop(1, ntp, lambda j: hand_copy(w, j).start())
+    def sp_of(to_z, to_y):
+        return (to_z * ny + to_y) * nt + t
+
+    def z_of(j):
+        return lax.rem(z + j, nz)
+
+    def y_of(j):
+        return lax.rem(y + j, ny)
+
+    def share_copy(j):
+        slot = w * ntp + c
+        return remote(xg.at[slot], xg.at[slot], ag_s.at[j], ag_r.at[slot], sp_of(z_of(j), y), c)
+
+    def over_y(from_z, j):
+        slot = (from_z * ny + y) * ntp + c
+        return remote(xg.at[slot], xg.at[slot], yf_s.at[from_z * ny + j], ag_r.at[slot],
+                      sp_of(z, y_of(j)), c)
 
     def slot_wait(slot):
-        remote(xg.at[slot], xg.at[slot], ag_s.at[0], ag_r.at[slot], s, c).wait_recv()
-
-    own_up.wait()
+        remote(xg.at[slot], xg.at[slot], ag_s.at[0], ag_r.at[slot], peer(1), c).wait_recv()
+
+    def pass_on(from_z):
+        loop(1, ny, lambda i: over_y(from_z, i).start())
+        loop(1, ntp, lambda i: hand_copy(from_z * ny + y, i).start())
+
+    def arrive(j):
+        from_z = z_of(nz - j)
+        slot_wait((from_z * ny + y) * ntp + c)
+        pass_on(from_z)
+
+    loop(1, nz, lambda j: share_copy(j).start())
+    pass_on(z)
+
     own_dn.wait()
-
-    def weight_waits(j):
-        source = peer(j)
-        remote(up_part(w), up_rows(source), up_s.at[j], up_r.at[source], source, c).wait_recv()
-        remote(dn_part(w), dn_slab.at[source], dn_s.at[j], dn_r.at[source], source, c).wait_recv()
+    loop(1, nt, lambda i: dn_hand(0, i).start())
+    loop(1, nw, dn_pass)
+
+    def other_waits(j):
+        source = (j // (nt - 1)) * nt + lax.rem(t + 1 + lax.rem(j, nt - 1), nt)
+        up_wait(source)
+        dn_wait(source)
 
     joined = max(1, 256 // depth)
-
-    def arrive(j):
-        from_w = group(nw - j)
-        slot_wait(from_w * ntp + c)
-        loop(1, ntp, lambda i: hand_copy(from_w, i).start())
 
     def tp_copy(to_w, j):
         to = mate(j)
         return remote(pbuf.at[to_w, own_block(to), :], tp_in.at[to_w, c],
                       tp_s.at[to_w * ntp + j], tp_r.at[to_w * ntp + c], s, to)
 
-    def mixer_step(j):
-        from_w = group(nw - j)
+    def mixer_step(from_w):
         loop(1, ntp, lambda i: slot_wait(from_w * ntp + mate(i)))
         rows = xg[pl.ds(from_w * ntp, ntp)].reshape(ntp * own, xg.shape[2])
         hidden = jnp.square(jnp.maximum(dot(rows, up_slab[...]), 0.0)).astype(BF16)
@@ -331,11 +376,7 @@
             pbuf[from_w, :, a * depth:(a + joined) * depth] = dot(hidden, block).astype(BF16)
         loop(1, ntp, lambda i: tp_copy(from_w, i).start())
 
-    def sum_copy(to_w, j):
-        return remote(rs_out.at[to_w], rs_in.at[w], rs_s.at[j], rs_r.at[w], to_w * nt + t, c)
-
-    def pair_sum(j):
-        to_w = group(nw - j)
+    def pair_sum(to_w):
         for i in range(1, ntp):
             source = mate(i)
             remote(pbuf.at[to_w, own_block(c), :], tp_in.at[to_w, source],
@@ -343,22 +384,60 @@
         added = pbuf[to_w, own_block(c), :].astype(F32)
         for i in range(1, ntp):
             added = added + tp_in[to_w, mate(i)].astype(F32)
-        return to_w, added.astype(BF16)
+        return added
+
+    def y_copy(to_z, j):
+        to = y_of(j)
+        return remote(y_out.at[to_z * ny + to], y_in.at[to_z * ny + y],
+                      yr_s.at[to_z * ny + j], yr_r.at[to_z * ny + y], sp_of(z, to), c)
+
+    def sum_copy(to_z, j):
+        return remote(rs_out.at[to_z], rs_in.at[z], rs_s.at[j], rs_r.at[z], sp_of(to_z, y), c)
+
+    def compute(j):
+        at = z_of(nz - j)
+
+        def other(i):
+            slot = (at * ny + y_of(i)) * ntp + c
+            slot_wait(slot)
+            loop(1, ntp, lambda k: hand_copy(at * ny + y_of(i), k).start())
+
+        loop(1, ny, other)
+        mixer_step(at * ny + y)
+
+        def other_step(i):
+            to = at * ny + y_of(i)
+            mixer_step(to)
+            y_out[to] = pair_sum(to).astype(BF16)
+            y_copy(at, i).start()
+
+        loop(1, ny, other_step)
+
+    def collect(j):
+        at = z_of(nz - j)
+        added = pair_sum(at * ny + y)
+        for i in range(1, ny):
+            source = at * ny + y_of(i)
+            remote(y_out.at[source], y_in.at[source], yr_s.at[0], yr_r.at[source],
+                   peer(1), c).wait_recv()
+            added = added + y_in[source].astype(F32)
+        return at, added.astype(BF16)
 
     def send_sum(j):
-        to_w, added = pair_sum(j)
-        rs_out[to_w] = added
-        sum_copy(to_w, j).start()
-
-    loop(1, ns, weight_waits)
-    arrive(1)
+        to_z, added = collect(j)
+        rs_out[to_z] = added
+        sum_copy(to_z, j).start()
+
+    if nz > 1:
+        arrive(1)
+    loop(0, nw * (nt - 1), other_waits)
 
     def step(j, carry):
-        @pl.when(j < nw - 1)
+        @pl.when(j < nz - 1)
         def _():
             arrive(j + 1)
 
-        mixer_step(j)
+        compute(j)
 
         @pl.when(j > 1)
         def _():
@@ -366,27 +445,26 @@
 
         return carry
 
-    lax.fori_loop(1, nw, step, 0)
-    mixer_step(nw)
-    send_sum(nw - 1)
-    _, added = pair_sum(nw)
-    rs_in[w] = added
+    lax.fori_loop(1, nz, step, 0)
+    compute(nz)
+    if nz > 1:
+        send_sum(nz - 1)
+    _, added = collect(nz)
+    rs_in[z] = added
 
     def sum_wait(j):
-        source = group(j)
+        source = z_of(j)
         remote(rs_out.at[source], rs_in.at[source], rs_s.at[j], rs_r.at[source],
-               source * nt + t, c).wait_recv()
-
-    loop(1, nw, sum_wait)
+               peer(1), c).wait_recv()
+
+    loop(1, nz, sum_wait)
     mlp_out = rs_in[0].astype(F32)
-    for i in range(1, nw):
+    for i in range(1, nz):
         mlp_out = mlp_out + rs_in[i].astype(F32)
     mlp_out = mlp_out.astype(BF16).astype(F32)
     out[...] = layer_norm(xg[w * ntp + c].astype(F32) + mlp_out, outg[...]).astype(BF16)
 
     def drain(j):
-        up_copy(j).wait_send()
-        dn_copy(j).wait_send()
         small_copy(j).wait_send()
         state_copy(j).wait_send()
         back_copy(j).wait_send()
@@ -394,11 +472,31 @@
     loop(1, ns, drain)
     loop(1, ntp, lambda j: mix_copy(j).wait_send())
 
+    def drain_weights(j):
+        up_copy(j).wait_send()
+        dn_copy(j).wait_send()
+
+    loop(1, nw, drain_weights)
+
+    def drain_hand(j):
+        for i in range(1, nt):
+            up_hand(j, i).wait_send()
+            dn_hand(j, i).wait_send()
+
+    loop(0, nw, drain_hand)
+
     def drain_group(j):
         share_copy(j).wait_send()
-        sum_copy(group(nw - j), j).wait_send()
-
-    loop(1, nw, drain_group)
+        sum_copy(z_of(nz - j), j).wait_send()
+
+    loop(1, nz, drain_group)
+
+    def drain_y(a):
+        for j in range(1, ny):
+            over_y(a, j).wait_send()
+            y_copy(a, j).wait_send()
+
+    loop(0, nz, drain_y)
 
     def drain_pair(a):
         for j in range(1, ntp):
@@ -415,6 +513,7 @@
     while (up.shape[1] // (ns // nt)) % 128:
         nt *= 2
     nw = ns // nt
+    ny = 2 if nw % 2 == 0 else 1
     width = up.shape[1] // nw
     depth = up.shape[0]
     length, model = stream.shape
@@ -428,7 +527,7 @@
     hbm = pl.BlockSpec(memory_space=pl.ANY)
     sem = pltpu.SemaphoreType.DMA
     return pl.pallas_call(
-        functools.partial(kernel, ns, ntp, nt, ns // 2),
+        functools.partial(kernel, ns, ntp, nt, ny),
         out_shape=jax.ShapeDtypeStruct((own, model), BF16),
         in_specs=[vm] * 9 + [hbm, vm, vm, hbm, hbm, vm],
         out_specs=vm,
@@ -452,9 +551,11 @@
             pltpu.VMEM((nw, ntp, own, model), BF16),
             pltpu.VMEM((nw, own, model), BF16),
             pltpu.VMEM((nw, own, model), BF16),
+            pltpu.VMEM((nw // ny, own, model), BF16),
+            pltpu.VMEM((nw // ny, own, model), BF16),
             sem((3,)),
-        ] + [sem((ns,))] * 10 + [sem((ntp,))] * 2 + [
-            sem((nw,)), sem((nw * ntp,)), sem((nw * ntp,)), sem((nw * ntp,)),
+        ] + [sem((ns,))] * 12 + [sem((ntp,))] * 2 + [
+            sem((nw,)), sem((nw,)), sem((nw,)), sem((nw,)), sem((nw * ntp,)), sem((nw * ntp,)), sem((nw * ntp,)),
             sem((nw * ntp,)), sem((nw,)), sem((nw,)),
         ],
         compiler_params=pltpu.CompilerParams(

time: 233 us -> 146 us (0.63)
  Pallas kernels: 231 us -> 145 us
    pallas_call x1, Pallas kernels: 231 us -> 145 us  [body(): pl.pallas_call(functools.partial(kernel, ns, ntp, nt, ny), out_shape=jax....]
where the time goes in v2:
time: 146 us
  Pallas kernels  145 us (99%)
  local copies, waits for them, and re-layouts  1.67 us (1%)
    pallas_call x1, Pallas kernels, body(): pl.pallas_call(functools.partial(kernel, ns, ntp, nt, ny), out_shape=jax....  145 us

profile of v2, /device:TPU:0, one launch (start us, length us, event | category | flops | bytes accessed | tf_op | source)
XLA Modules:
  0.0 146.3 jit_solution(5453424864454773942)
XLA Ops:
  0.0 144.6 %shard_map.145 = bf16[64,2048]{1,0:T(8,128)(2,1)} custom-call(bf16[128,512]{1,0:T(8,128)(2,1)} %q1.1, bf16[128,512]{1,0:T(8,128)(2,1)} %k1.1, bf16[128,256]{1,0:T(8,128)(2,1)} %q2.1, bf16[128,256]{1,0:T(8,128)(2,1)} %k2.1, bf16[128,1024]{1,0:T(8,128)(2,1)} %v.1, bf16[128,1024]{1,0:T(8,128)(2,1)} %og.1, f32[8,128]{1,0:T(8,128)} %ig.1, f32[8,128]{1,0:T(8,128)} %fg.1, ...), custom_call_target="tpu_custom_call" | custom-call | tf_op jit(solution)/shard_map/pallas_call | solution.py:529
  144.6 1.7 %copy.17 = bf16[64,2048]{1,0:T(8,128)(2,1)} copy(bf16[64,2048]{1,0:T(8,128)(2,1)} %shard_map.145) | data formatting | bytes 524288
